TPU v7x, 512 devices: a whole 4x4x16 slice. The times are simulated.
512 devices in a mesh: sp: 16 (over y, x), tp: 32 (over z, core).
Axes of the slice: x: 4, y: 4, z: 16, core: 2. Of those that a mesh axis runs over, the one named last changes fastest.
Arguments:
- tokens: bfloat16 [3, 8192, 4096], P(None, 'sp', 'tp'), may hold values from -6 to 6
- new_token: bfloat16 [3, 1, 4096], P(None, None, 'tp'), may hold values from -6 to 6
- query_weight: bfloat16 [4096, 4096], P(None, 'tp'), may hold values from -0.09375 to 0.09375
- key_weight: bfloat16 [4096, 4096], P(None, 'tp'), may hold values from -0.09375 to 0.09375
- value_weight: bfloat16 [4096, 4096], P(None, 'tp'), may hold values from -0.09375 to 0.09375
- log_decay: float32 [64], P('tp'), may hold values from -0.034 to 0
Outputs:
- state: bfloat16 [3, 64, 64, 64], P(None, 'tp', 'sp')
- read: bfloat16 [3, 4096], P(None, 'tp')
All inputs are finite; a program needn't handle non-finite values.
Results may differ from a plain program's by a relative error of at most 0.012.
Values may be sent and summed in bfloat16 or wider, within the bound.
A program may use at most 64 MiB of HBM per device.

v0:
```python
import jax
import jax.numpy as jnp
from jax import lax
from jax.sharding import PartitionSpec as P

HD = 64


def cut_along(value, dim, count):
    dims = value.shape
    tiles = value.reshape(*dims[:dim], count, dims[dim] // count, *dims[dim + 1 :])
    return jnp.moveaxis(tiles, dim, 0)


def sent_and_summed(value, axis, dim):
    tiles = cut_along(value, dim, lax.axis_size(axis))
    arrived = lax.all_to_all(tiles, axis, split_axis=0, concat_axis=0, tiled=True)
    return arrived.sum(axis=0)


def from_everyone(value, axis):
    copies = jnp.broadcast_to(value, (lax.axis_size(axis), *value.shape))
    return lax.all_to_all(copies, axis, split_axis=0, concat_axis=0, tiled=True)


def over_copies(value, axis):
    everything = from_everyone(value, axis)
    return jnp.sum(everything, axis=0)


def rotate(values, positions):
    half_dim = values.shape[-1] // 2
    inverse = 10000.0 ** (-jnp.arange(half_dim, dtype=jnp.float32) / half_dim)
    angles = positions.astype(jnp.float32)[:, None, None] * inverse[None, None, :]
    cosine = jnp.cos(angles)
    sine_part = jnp.sin(angles)
    first = values[..., :half_dim]
    second = values[..., half_dim:]
    return jnp.concatenate(
        [first * cosine - second * sine_part, first * sine_part + second * cosine], axis=-1
    )


def group_norm(output):
    centered = output - jnp.mean(output, axis=-1, keepdims=True)
    return centered * lax.rsqrt(jnp.mean(centered * centered, axis=-1, keepdims=True) + 1e-05)


def body(tokens, new_token, query_weight, key_weight, value_weight, log_decay):
    sequences, span_len, _ = tokens.shape
    head_count = log_decay.shape[0]
    inner = head_count * HD
    groups = lax.axis_size("sp")
    own_index = lax.axis_index("sp")
    key_scale = HD ** (-0.5)
    row_weights = jnp.concatenate([key_weight, value_weight], axis=1)
    all_weights = jnp.concatenate([key_weight, value_weight, query_weight], axis=1)
    row_piece = lax.all_gather(tokens, "tp", axis=2, tiled=True)
    new_piece = lax.all_gather(new_token, "tp", axis=2, tiled=True)
    row_total = jnp.dot(row_piece, row_weights, preferred_element_type=jnp.float32)
    new_total = jnp.dot(new_piece, all_weights, preferred_element_type=jnp.float32)
    row_total = row_total.reshape(sequences, span_len, 2, head_count, HD)
    offsets = own_index * span_len + jnp.arange(span_len, dtype=jnp.int32)
    key_rows = (rotate(row_total[:, :, 0], offsets) * key_scale).astype(jnp.bfloat16)
    value_rows = row_total[:, :, 1].astype(jnp.bfloat16)
    to_end = (span_len - 1 - jnp.arange(span_len, dtype=jnp.int32)).astype(jnp.float32)
    decay_rows = jnp.exp(to_end[:, None] * log_decay[None, :])
    weighted = (key_rows.astype(jnp.float32) * decay_rows[None, :, :, None]).astype(jnp.bfloat16)
    span_state = jnp.einsum(
        "sthk,sthv->shkv", weighted, value_rows, preferred_element_type=jnp.float32
    )
    carried_state = jnp.exp(log_decay * (span_len * (groups - 1 - own_index)).astype(jnp.float32))
    scaled_state = span_state * carried_state[None, :, None, None]
    state_rows = sent_and_summed(scaled_state, "sp", 2)
    new_total = new_total.reshape(sequences, 1, 3, head_count, HD)
    new_position = jnp.full((1,), groups * span_len, jnp.int32)
    fresh_key = (rotate(new_total[:, :, 0], new_position) * key_scale).astype(jnp.bfloat16)[:, 0]
    new_value = new_total[:, 0, 1].astype(jnp.bfloat16)
    new_query = rotate(new_total[:, :, 2], new_position).astype(jnp.bfloat16)[:, 0]
    query_entries = new_query.astype(jnp.float32)
    decay_one = jnp.exp(log_decay)[None, :, None]
    partial_read = (
        jnp.einsum("shkv,shk->shv", scaled_state, query_entries, precision=lax.Precision.HIGHEST)
        * decay_one
    )
    summed = over_copies(partial_read, "sp")
    own_term = jnp.sum(
        query_entries * fresh_key.astype(jnp.float32), axis=-1, keepdims=True
    ) * new_value.astype(jnp.float32)
    normed = group_norm(summed + own_term)
    return (state_rows.astype(jnp.bfloat16), normed.reshape(sequences, inner).astype(jnp.bfloat16))


def solution(mesh):
    return jax.shard_map(
        body,
        mesh=mesh,
        in_specs=(
            P(None, "sp", "tp"),
            P(None, None, "tp"),
            P(None, "tp"),
            P(None, "tp"),
            P(None, "tp"),
            P("tp"),
        ),
        out_specs=(P(None, "tp", "sp", None), P(None, "tp")),
        check_vma=False,
    )
```

profile of v0, /device:TPU:1, one launch (start us, length us, event | category | flops | bytes accessed | tf_op | source)
XLA Modules:
  0.0 171.5 jit_solution(1786247637780565341)
XLA Ops:
  7.2 0.0 copy-start
  7.2 0.0 copy-start.1
  7.2 0.0 copy-start.3
  7.2 0.0 all-gather.2.cloned.1.call-start
  7.2 0.7 all-gather.2.cloned.1.call-update
  7.9 1.5 copy.27
  9.4 0.0 copy-done.1
  9.4 1.4 copy.26
  10.8 37.7 %all_gather.7 = bf16[3,1,4096]{2,0,1:T(4,128)(2,1)S(1)} all-gather(bf16[3,1,128]{2,0,1:T(4,128)(2,1)S(1)} %copy-done.3), channel_id=1, replica_groups=mesh['sp'=16,'tp'=32] {'tp'}, dimensions={2}, use_global_device_ids=true | all-gather | bytes 25344 | tf_op jit(solution)/shard_map/all_gather | solution.py:59
  48.5 0.0 copy-done
  48.5 1.8 %fusion.9 = f32[3,384]{1,0:T(4,128)S(1)} fusion(bf16[4096,128]{1,0:T(8,128)(2,1)} %param.8, bf16[4096,128]{1,0:T(8,128)(2,1)S(1)} %copy-done, bf16[4096,128]{1,0:T(8,128)(2,1)S(1)} %copy-done.1, bf16[3,1,4096]{2,0,1:T(4,128)(2,1)S(1)} %all_gather.7), kind=kOutput, calls=%fused_computation.11 | convolution fusion | flops 18874368 | bytes 3174912 | tf_op jit(solution)/shard_map/dot_general | solution.py:61
  50.3 0.1 reshape.207
  50.4 0.1 multiply_sine_fusion.1
  50.4 0.1 subtract_bitcast_fusion
  50.5 0.1 fusion.31
  50.6 0.1 multiply_exponential_fusion
  50.7 0.3 multiply_cosine_fusion
  51.0 79.8 %all-gather.2.cloned.1.call-done = bf16[3,512,4096]{2,1,0:T(8,128)(2,1)} async-done(((bf16[3,512,128]{2,1,0:T(8,128)(2,1)}), bf16[3,512,4096]{2,1,0:T(8,128)(2,1)}) %all-gather.2.cloned.1.call-update) | async-done | bytes 12582928 | tf_op jit(solution)/shard_map/all_gather | solution.py:58
  130.8 6.8 %fusion.6 = f32[256,3,512]{2,0,1:T(8,128)S(1)} fusion(bf16[3,512,4096]{2,1,0:T(8,128)(2,1)} %all-gather.2.cloned.1.call-done, bf16[4096,128]{0,1:T(8,128)(2,1)S(1)} %copy.27, bf16[4096,128]{0,1:T(8,128)(2,1)} %copy.26), kind=kOutput, calls=%fused_computation.7 | convolution fusion | flops 3225419776 | bytes 16252928 | tf_op jit(solution)/shard_map/dot_general | solution.py:60
  137.6 0.1 copy_bitcast_fusion
  137.7 0.1 multiply_subtract_fusion
  137.8 0.3 convolution_multiply_fusion
  138.1 0.2 fusion.22
  138.3 0.1 broadcast_multiply_fusion
  138.4 0.7 reshape.215
  139.1 7.3 %all-to-all-start.1 = ((f32[16,1,384]{2,1,0:T(1,128)}), f32[16,1,384]{2,1,0:T(1,128)S(1)}, u32[]{:S(2)}, u32[]{:S(2)}) async-start(f32[16,1,384]{2,1,0:T(1,128)} %reshape.215), calls=%async_computation.1 | async-start | bytes 49152 | tf_op jit(solution)/shard_map/all_to_all | solution.py:23
  146.4 0.2 multiply_reduce_fusion.1
  146.6 0.1 mul.279
  146.6 0.1 mul.280
  146.7 0.1 reshape.208
  146.8 0.8 reshape.213
  147.7 5.2 %all-to-all-done.1 = f32[16,1,384]{2,1,0:T(1,128)S(1)} async-done(((f32[16,1,384]{2,1,0:T(1,128)}), f32[16,1,384]{2,1,0:T(1,128)S(1)}, u32[]{:S(2)}, u32[]{:S(2)}) %all-to-all-start.1) | async-done | bytes 24608 | tf_op jit(solution)/shard_map/all_to_all | solution.py:23
  152.8 3.5 %all-to-all-start = ((f32[16,1,1536]{2,1,0:T(1,128)}), f32[16,1,1536]{2,1,0:T(1,128)S(1)}, u32[]{:S(2)}, u32[]{:S(2)}) async-start(f32[16,1,1536]{2,1,0:T(1,128)} %reshape.213), calls=%async_computation | async-start | bytes 196608 | tf_op jit(solution)/shard_map/all_to_all | solution.py:17
  156.4 0.5 broadcast.164
  156.9 0.7 reduce.1
  157.6 0.1 reshape.216
  157.7 0.2 fusion.32
  157.9 0.1 reduce_sum.49
  158.0 0.2 multiply_reduce_fusion
  158.1 0.1 mul.284
  158.2 0.1 mul.285
  158.3 0.1 sub.41
  158.4 0.1 sub.42
  158.4 0.6 multiply_convert_fusion.2
  159.0 4.0 %all-to-all-done = f32[16,1,1536]{2,1,0:T(1,128)S(1)} async-done(((f32[16,1,1536]{2,1,0:T(1,128)}), f32[16,1,1536]{2,1,0:T(1,128)S(1)}, u32[]{:S(2)}, u32[]{:S(2)}) %all-to-all-start) | async-done | bytes 98336 | tf_op jit(solution)/shard_map/all_to_all | solution.py:17
  163.0 0.9 reduce
  163.9 0.1 reshape.214
  164.0 0.7 reduce_sum.47
  (14 shorter events, 0.2 us)
Async XLA Ops:
  7.2 41.3 %copy-start = (bf16[4096,128]{1,0:T(8,128)(2,1)S(1)}, bf16[4096,128]{1,0:T(8,128)(2,1)}, u32[]{:S(2)}) copy-start(bf16[4096,128]{1,0:T(8,128)(2,1)} %param.10) | copy-start | bytes 3145732
  7.2 2.3 %copy-start.1 = (bf16[4096,128]{1,0:T(8,128)(2,1)S(1)}, bf16[4096,128]{1,0:T(8,128)(2,1)}, u32[]{:S(2)}) copy-start(bf16[4096,128]{1,0:T(8,128)(2,1)} %param.9) | copy-start | bytes 3145732
  7.2 3.6 %copy-start.3 = (bf16[3,1,128]{2,0,1:T(4,128)(2,1)S(1)}, bf16[3,1,128]{2,0,1:T(4,128)(2,1)}, u32[]{:S(2)}) copy-start(bf16[3,1,128]{2,0,1:T(4,128)(2,1)} %param.7) | copy-start | bytes 2308
  7.2 123.6 %all-gather.2.cloned.1.call-start = ((), (), s32[]{:S(2)}) async-start(), calls=%async_computation.2 | async-start | bytes 12976128 | tf_op jit(solution)/shard_map/all_gather | solution.py:58
  48.5 2.1 %copy-start.2 = (f32[2]{0:T(128)S(1)}, f32[2]{0:T(128)}, u32[]{:S(2)}) copy-start(f32[2]{0:T(128)} %param.11) | copy-start | bytes 28
  139.1 13.7 %all-to-all-start.1 = ((f32[16,1,384]{2,1,0:T(1,128)}), f32[16,1,384]{2,1,0:T(1,128)S(1)}, u32[]{:S(2)}, u32[]{:S(2)}) async-start(f32[16,1,384]{2,1,0:T(1,128)} %reshape.215), calls=%async_computation.1 | async-start | bytes 49152 | tf_op jit(solution)/shard_map/all_to_all | solution.py:23
  152.8 10.1 %all-to-all-start = ((f32[16,1,1536]{2,1,0:T(1,128)}), f32[16,1,1536]{2,1,0:T(1,128)S(1)}, u32[]{:S(2)}, u32[]{:S(2)}) async-start(f32[16,1,1536]{2,1,0:T(1,128)} %reshape.213), calls=%async_computation | async-start | bytes 196608 | tf_op jit(solution)/shard_map/all_to_all | solution.py:17
Sparse Core Ops, SparseCore 0:
  10.0 120.7 all-gather.1
where the time goes:
time: 173 us; the launch traced here: 172 us
  waiting for transfers between devices  89.6 us (52%)
  blocking collectives  37.7 us (22%)
  between operations  14.2 us (8%)
  starting transfers between devices  10.8 us (6%)
  matrix products  9.01 us (5%)
  local copies, waits for them, and re-layouts  5.97 us (3%)
  other arithmetic  4.18 us (2%)
    all_gather x1, waiting for transfers between devices, body(): row_piece = lax.all_gather(tokens, 'tp', axis=2, tiled=True)  79.8 us
    all_gather x1, blocking collectives, body(): new_piece = lax.all_gather(new_token, 'tp', axis=2, tiled=True)  37.7 us
    all_to_all x1, starting transfers between devices, from_everyone(): return lax.all_to_all(copies, axis, split_axis=0, concat_axis=0, tiled=True)  7.27 us
    dot_general x1, matrix products, body(): jnp.dot(row_piece, row_weights, preferred_element_type=jnp.float32)  6.76 us
    all_to_all x1, waiting for transfers between devices, from_everyone(): return lax.all_to_all(copies, axis, split_axis=0, concat_axis=0, tiled=True)  5.18 us
    unnamed x14, local copies, waits for them, and re-layouts  4.6 us
    all_to_all x1, waiting for transfers between devices, sent_and_summed(): lax.all_to_all(tiles, axis, split_axis=0, concat_axis=0, tiled=True)  3.96 us
    all_to_all x1, starting transfers between devices, sent_and_summed(): lax.all_to_all(tiles, axis, split_axis=0, concat_axis=0, tiled=True)  3.51 us
  transfers between devices with their start and end apart: 3, of which 3 were waited for; matrix products, arithmetic and copies ran while one was open for 5% of the time, Pallas kernels for 0%

commit v1 on v0

v1 whole, which is shorter than its diff:
```python
import functools

import jax
import jax.numpy as jnp
import numpy as np
from jax import lax
from jax.experimental import pallas as pl
from jax.experimental.pallas import tpu as pltpu
from jax.sharding import PartitionSpec as P

HD = 64
MESH = pl.DeviceIdType.MESH
NZ = 16
CH = 256
NCH = 6
HALF = 3
STEPS = 7 * NCH + HALF
LANES = 128


def kernel(
    groups,
    tok_ref,
    new_ref,
    wq_ref,
    wk_ref,
    wv_ref,
    ld_ref,
    state_ref,
    read_ref,
    blocks,
    news,
    weights,
    acc,
    acc_new,
    cos_t,
    sin_t,
    dec_t,
    out_buf,
    in_buf,
    tok_sem,
    w_sem,
    up_send,
    dn_send,
    pt_send,
    up_recv,
    dn_recv,
    pu_recv,
    pd_recv,
    own_recv,
    nu_send,
    nd_send,
    np_send,
    nu_recv,
    nd_recv,
    npu_recv,
    npd_recv,
    nown_recv,
    x_send,
    x_recv,
):
    sp = lax.axis_index("sp")
    tp = lax.axis_index("tp")
    z = tp // 2
    core = tp % 2
    up = ((z + 1) % NZ) * 2 + core
    dn = ((z + NZ - 1) % NZ) * 2 + core
    partner = z * 2 + (1 - core)
    span = NCH // 3 * CH

    own_copies = []
    for ch in range(NCH):
        half, p = ch // 3, ch % 3
        c = pltpu.make_async_copy(
            tok_ref.at[p, pl.ds(half * CH, CH), :], blocks.at[tp * NCH + ch], tok_sem.at[ch]
        )
        c.start()
        own_copies.append(c)
    w_copies = []
    for i, ref in enumerate((wk_ref, wv_ref, wq_ref)):
        c = pltpu.make_async_copy(ref, weights.at[:, pl.ds(i * LANES, LANES)], w_sem.at[i])
        c.start()
        w_copies.append(c)

    barrier = pltpu.get_barrier_semaphore()
    for peer in (up, dn, partner):
        pl.semaphore_signal(barrier, inc=1, device_id=(sp, peer), device_id_type=MESH)
    for d in range(1, groups):
        pl.semaphore_signal(
            barrier, inc=1, device_id=((sp + d) % groups, tp), device_id_type=MESH
        )

    own_new = jnp.concatenate(
        [new_ref[:, 0, :].astype(jnp.float32), jnp.zeros((13, LANES), jnp.float32)], axis=0
    )
    news[tp] = own_new.astype(jnp.bfloat16)

    pl.semaphore_wait(barrier, 3 + groups - 1)

    def remote(src, send, recv, peer, ref=None):
        ref = blocks if ref is None else ref
        return pltpu.make_async_remote_copy(
            src_ref=ref.at[src],
            dst_ref=ref.at[src],
            send_sem=send,
            recv_sem=recv,
            device_id=(sp, peer),
            device_id_type=MESH,
        )

    remote(tp, nu_send.at[0], nu_recv.at[0], up, news).start()
    remote(tp, nd_send.at[0], nd_recv.at[0], dn, news).start()
    remote(tp, np_send.at[15], nown_recv, partner, news).start()
    for ch in range(NCH):
        own_copies[ch].wait()
    for pos in range(NCH):
        cu, cd = pos, (pos + HALF) % NCH
        remote(tp * NCH + cu, up_send, up_recv.at[pos], up).start()
        remote(tp * NCH + cd, dn_send, dn_recv.at[pos], dn).start()
    for ch in range(NCH):
        remote(tp * NCH + ch, pt_send, own_recv.at[ch], partner).start()

    def source(t, down):
        k, pos = t // NCH, t % NCH
        if down:
            sz = (z + 1 + k) % NZ
            ch = (pos + HALF) % NCH
        else:
            sz = (z + NZ - 1 - k) % NZ
            ch = pos
        return k, sz, ch

    lane = lax.broadcasted_iota(jnp.int32, (1, LANES), 1)
    inverse = jnp.zeros((1, LANES), jnp.float32)
    freq = (10000.0 ** (-np.arange(32, dtype=np.float64) / 32)).astype(np.float32)
    for i in range(32):
        inverse = jnp.where(lane % 32 == i, float(freq[i]), inverse)
    first = (lane % HD) < 32
    low = lane < HD
    ld = jnp.where(low, ld_ref[0], ld_ref[1])
    row = lax.broadcasted_iota(jnp.int32, (span, LANES), 0)
    angle = (row + sp * span).astype(jnp.float32) * inverse
    cos_t[...] = jnp.cos(angle) * 0.125
    sin_t[...] = jnp.where(first, -jnp.sin(angle), jnp.sin(angle)) * 0.125
    dec_t[...] = jnp.exp((span - 1 - row).astype(jnp.float32) * ld)
    carried = jnp.exp(ld * (span * (groups - 1 - sp)).astype(jnp.float32))

    for c in w_copies:
        c.wait()

    def lhs(sz, ch):
        return jnp.concatenate(
            [blocks[(2 * sz) * NCH + ch], blocks[(2 * sz + 1) * NCH + ch]], axis=1
        )

    def rows_of(sz):
        return pl.ds(pl.multiple_of(sz * 256, 256), 256)

    def new_dot(sz):
        x = jnp.concatenate([news[2 * sz], news[2 * sz + 1]], axis=1)
        return jnp.dot(x, weights[rows_of(sz), :], preferred_element_type=jnp.float32)

    def kv_dot(sz, ch):
        return jnp.dot(
            lhs(sz, ch), weights[rows_of(sz), 0:256], preferred_element_type=jnp.float32
        )

    remote(partner, np_send.at[15], nown_recv, partner, news).wait_recv()
    acc_new[...] = new_dot(z)
    for ch in range(NCH):
        remote(partner * NCH + ch, pt_send, own_recv.at[ch], partner).wait_recv()
        acc[pl.ds(ch * CH, CH), :] = kv_dot(z, ch)

    def relay(t):
        k, su, cu = source(t, False)
        _, sd, cd = source(t, True)
        bu = (su * 2 + core) * NCH + cu
        bd = (sd * 2 + core) * NCH + cd

        def small():
            nu = su * 2 + core
            nd = sd * 2 + core
            remote(nu, nu_send.at[k], nu_recv.at[k], up, news).wait_recv()

            @pl.when(k < 7)
            def _():
                remote(nu, nu_send.at[k + 1], nu_recv.at[k + 1], up, news).start()
                remote(nd, nd_send.at[k], nd_recv.at[k], dn, news).wait_recv()

                @pl.when(k < 6)
                def _():
                    remote(nd, nd_send.at[k + 1], nd_recv.at[k + 1], dn, news).start()

                remote(nd, np_send.at[k + 8], npd_recv.at[k], partner, news).start()

            remote(nu, np_send.at[k], npu_recv.at[k], partner, news).start()

        if isinstance(t, int):
            if t % NCH == 0:
                small()
        else:
            pl.when(t % NCH == 0)(small)

        def forward():
            remote(bu, up_send, up_recv.at[t + NCH], up).start()

        def forward_down():
            remote(bd, dn_send, dn_recv.at[t + NCH], dn).start()

        remote(bu, up_send, up_recv.at[t], up).wait_recv()
        if isinstance(t, int):
            if t + NCH < STEPS:
                forward()
        else:
            pl.when(t + NCH < STEPS)(forward)
        remote(bu, pt_send, pu_recv.at[t], partner).start()
        remote(bd, dn_send, dn_recv.at[t], dn).wait_recv()
        if isinstance(t, int):
            if t + NCH < STEPS:
                forward_down()
        else:
            pl.when(t + NCH < STEPS)(forward_down)
        remote(bd, pt_send, pd_recv.at[t], partner).start()

    def compute(t):
        k, su, cu = source(t, False)
        _, sd, cd = source(t, True)
        pc = 1 - core

        def small():
            remote(su * 2 + pc, np_send.at[k], npu_recv.at[k], partner, news).wait_recv()
            acc_new[...] += new_dot(su)

            @pl.when(k < 7)
            def _():
                remote(sd * 2 + pc, np_send.at[k], npd_recv.at[k], partner, news).wait_recv()
                acc_new[...] += new_dot(sd)

        if isinstance(t, int):
            if t % NCH == 0:
                small()
        else:
            pl.when(t % NCH == 0)(small)
        remote((su * 2 + pc) * NCH + cu, pt_send, pu_recv.at[t], partner).wait_recv()
        at = pl.ds(pl.multiple_of(cu * CH, CH), CH)
        acc[at, :] += kv_dot(su, cu)
        remote((sd * 2 + pc) * NCH + cd, pt_send, pd_recv.at[t], partner).wait_recv()
        at = pl.ds(pl.multiple_of(cd * CH, CH), CH)
        acc[at, :] += kv_dot(sd, cd)

    last = STEPS - HALF

    def step(t, carry):
        relay(t)
        pl.when(t >= 1)(lambda: compute(t - 1))
        return carry

    lax.fori_loop(0, last + 1, step, 0)

    def turned(x, cosine, sine):
        swapped = jnp.where(first, pltpu.roll(x, LANES - 32, 1), pltpu.roll(x, 32, 1))
        return x * cosine + swapped * sine

    relay(last + 1)
    compute(last)

    new_angle = (groups * span) * inverse
    new_cos = jnp.cos(new_angle)
    new_sin = jnp.where(first, -jnp.sin(new_angle), jnp.sin(new_angle))
    new_k = (turned(acc_new[0:8, 0:128], new_cos, new_sin) * 0.125).astype(jnp.bfloat16)
    new_v = acc_new[0:8, 128:256].astype(jnp.bfloat16).astype(jnp.float32)
    new_q = turned(acc_new[0:8, 256:384], new_cos, new_sin).astype(jnp.bfloat16)
    new_q = new_q.astype(jnp.float32)
    product = new_q * new_k.astype(jnp.float32)

    def head_sums(x):
        lo = jnp.sum(jnp.where(low, x, 0.0), axis=1, keepdims=True)
        hi = jnp.sum(jnp.where(low, 0.0, x), axis=1, keepdims=True)
        return jnp.where(low, lo, hi)

    own_term = head_sums(product) * new_v
    q_cols = jnp.transpose(jnp.concatenate([new_q] * 16, axis=0))
    one = jnp.exp(ld)

    def finish(p):
        total = None
        for half in range(2):
            at = pl.ds(half * CH, CH)
            rows = acc[pl.ds((half * 3 + p) * CH, CH), :]
            keys = turned(rows[:, 0:128], cos_t[at, :], sin_t[at, :]).astype(jnp.bfloat16)
            keys = (keys.astype(jnp.float32) * dec_t[at, :]).astype(jnp.bfloat16)
            part = lax.dot_general(
                keys,
                rows[:, 128:256].astype(jnp.bfloat16),
                (((0,), (0,)), ((), ())),
                preferred_element_type=jnp.float32,
            )
            total = part if total is None else total + part
        tile = jnp.where(low, total[0:HD, :], total[HD:, :]) * carried
        query = jnp.where(low, q_cols[0:HD, p : p + 1], q_cols[HD:, p : p + 1])
        partial = jnp.sum(tile * query, axis=0, keepdims=True) * one
        out_buf[:, pl.ds(p * 4, 4), :] = tile.reshape(groups, HD // groups, LANES)
        out_buf[:, pl.ds(12 + p, 1), :] = jnp.broadcast_to(partial[None], (groups, 1, LANES))

    out_buf[:, pl.ds(15, 1), :] = jnp.zeros((groups, 1, LANES), jnp.float32)
    finish(0)
    relay(last + 2)
    compute(last + 1)
    finish(1)
    compute(last + 2)
    finish(2)

    for d in range(1, groups):
        peer = (sp + d) % groups
        pltpu.make_async_remote_copy(
            src_ref=out_buf.at[peer],
            dst_ref=in_buf.at[sp],
            send_sem=x_send,
            recv_sem=x_recv,
            device_id=(peer, tp),
            device_id_type=MESH,
        ).start()
    pltpu.make_async_copy(
        in_buf.at[pl.ds(0, groups - 1)], in_buf.at[pl.ds(0, groups - 1)], x_recv
    ).wait()
    in_buf[sp] = out_buf[sp]
    whole = in_buf[0]
    for d in range(1, groups):
        whole = whole + in_buf[d]

    for p in range(3):
        rows = whole[p * 4 : p * 4 + 4, :].astype(jnp.bfloat16)
        state_ref[p, 0] = rows[:, 0:HD]
        state_ref[p, 1] = rows[:, HD:]
    raw = whole[12:15, :] + own_term[0:3, :]
    centered = raw - head_sums(raw) * (1.0 / HD)
    scale = lax.rsqrt(head_sums(centered * centered) * (1.0 / HD) + 1e-05)
    read_ref[...] = (centered * scale).astype(jnp.bfloat16)

    def drain(view, sem):
        pltpu.make_async_copy(view, view, sem).wait()

    drain(blocks.at[pl.ds(0, STEPS)], up_send)
    drain(blocks.at[pl.ds(0, STEPS)], dn_send)
    drain(blocks.at[pl.ds(0, 2 * STEPS + NCH)], pt_send)
    for k in range(8):
        drain(news.at[0], nu_send.at[k])
    for k in range(7):
        drain(news.at[0], nd_send.at[k])
    for k in range(16):
        drain(news.at[0], np_send.at[k])
    drain(in_buf.at[pl.ds(0, groups - 1)], x_send)


def body(tokens, new_token, query_weight, key_weight, value_weight, log_decay):
    groups = lax.axis_size("sp")
    n_tp = lax.axis_size("tp")
    depth = n_tp * LANES
    dma = pltpu.SemaphoreType.DMA
    anywhere = pl.BlockSpec(memory_space=pl.ANY)
    vmem = pl.BlockSpec(memory_space=pltpu.VMEM)
    return pl.pallas_call(
        functools.partial(kernel, groups),
        out_shape=(
            jax.ShapeDtypeStruct((3, 2, HD // groups, HD), jnp.bfloat16),
            jax.ShapeDtypeStruct((3, LANES), jnp.bfloat16),
        ),
        in_specs=[
            anywhere,
            vmem,
            anywhere,
            anywhere,
            anywhere,
            pl.BlockSpec(memory_space=pltpu.SMEM),
        ],
        out_specs=(vmem, vmem),
        scratch_shapes=[
            pltpu.VMEM((n_tp * NCH, CH, LANES), jnp.bfloat16),
            pltpu.VMEM((n_tp, 16, LANES), jnp.bfloat16),
            pltpu.VMEM((depth, 3 * LANES), jnp.bfloat16),
            pltpu.VMEM((NCH * CH, 2 * LANES), jnp.float32),
            pltpu.VMEM((16, 3 * LANES), jnp.float32),
            pltpu.VMEM((2 * CH, LANES), jnp.float32),
            pltpu.VMEM((2 * CH, LANES), jnp.float32),
            pltpu.VMEM((2 * CH, LANES), jnp.float32),
            pltpu.VMEM((groups, 16, LANES), jnp.float32),
            pltpu.VMEM((groups, 16, LANES), jnp.float32),
            dma((NCH,)),
            dma((3,)),
            dma,
            dma,
            dma,
            dma((STEPS,)),
            dma((STEPS,)),
            dma((STEPS,)),
            dma((STEPS,)),
            dma((NCH,)),
            dma((8,)),
            dma((7,)),
            dma((16,)),
            dma((8,)),
            dma((7,)),
            dma((8,)),
            dma((7,)),
            dma,
            dma,
            dma,
        ],
        compiler_params=pltpu.CompilerParams(
            collective_id=0, has_side_effects=True, vmem_limit_bytes=48 * 1024 * 1024
        ),
    )(tokens, new_token, query_weight, key_weight, value_weight, log_decay)


def solution(mesh):
    return jax.shard_map(
        body,
        mesh=mesh,
        in_specs=(
            P(None, "sp", "tp"),
            P(None, None, "tp"),
            P(None, "tp"),
            P(None, "tp"),
            P(None, "tp"),
            P("tp"),
        ),
        out_specs=(P(None, "tp", "sp", None), P(None, "tp")),
        check_vma=False,
    )
```

time: 173 us -> 98.4 us (0.57)
  Pallas kernels: 0 us -> 90.9 us
  waiting for transfers between devices: 89.6 us -> 0 us
  blocking collectives: 37.7 us -> 0 us
  between operations: 14.2 us -> 0.65 us
  starting transfers between devices: 10.8 us -> 0 us
  matrix products: 9.01 us -> 0 us
  other arithmetic: 4.18 us -> 0 us
    pallas_call x0 -> x1, Pallas kernels: none -> 90.9 us  [body(): pl.pallas_call(functools.partial(kernel, groups), out_shape=(jax.ShapeDty...]
    all_gather x1 -> x0, waiting for transfers between devices: 79.8 us -> none  [body(): row_piece = lax.all_gather(tokens, 'tp', axis=2, tiled=True)]
    all_gather x1 -> x0, blocking collectives: 37.7 us -> none  [body(): new_piece = lax.all_gather(new_token, 'tp', axis=2, tiled=True)]
    all_to_all x2 -> x0, starting transfers between devices: 10.8 us -> none  [the longest x1 7.27 us: from_everyone(): return lax.all_to_all(copies, axis, split_axis=0, concat_axis=0, tiled=True)]
    all_to_all x2 -> x0, waiting for transfers between devices: 9.13 us -> none  [the longest x1 5.18 us: from_everyone(): return lax.all_to_all(copies, axis, split_axis=0, concat_axis=0, tiled=True)]
    dot_general x4 -> x0, matrix products: 9.01 us -> none  [the longest x1 6.76 us: body(): jnp.dot(row_piece, row_weights, preferred_element_type=jnp.float32)]
    unnamed x14 -> x13, local copies, waits for them, and re-layouts: 4.6 us -> 6.52 us
  transfers between devices with their start and end apart: 3 -> 0, of which waited for: 3 -> 0; matrix products, arithmetic and copies ran while one was open for 5% -> 0% of each run, Pallas kernels for 0% -> 0%
where the time goes in v1:
time: 98.4 us; the launch traced here: 98.1 us
  Pallas kernels  90.9 us (92%)
  local copies, waits for them, and re-layouts  6.52 us (7%)
    pallas_call x1, Pallas kernels, body(): pl.pallas_call(functools.partial(kernel, groups), out_shape=(jax.ShapeDty...  90.9 us
    unnamed x13, local copies, waits for them, and re-layouts  6.52 us

profile of v1, /device:TPU:1, one launch (start us, length us, event | category | flops | bytes accessed | tf_op | source)
XLA Modules:
  0.0 98.1 jit_solution(12481240405782900322)
XLA Ops:
  0.6 0.0 copy-start.4
  0.6 0.7 copy.8.new_ref
  1.3 0.0 copy-done.4
  1.3 0.0 copy-start
  1.3 1.2 %copy-done = bf16[4096,128]{1,0:T(8,128)(2,1)S(1)} copy-done((bf16[4096,128]{1,0:T(8,128)(2,1)S(1)}, bf16[4096,128]{1,0:T(8,128)(2,1)}, u32[]{:S(2)}) %copy-start) | copy-done | bytes 1048600
  2.6 0.0 copy-start.1
  2.6 1.2 %copy-done.1 = bf16[4096,128]{1,0:T(8,128)(2,1)S(1)} copy-done((bf16[4096,128]{1,0:T(8,128)(2,1)S(1)}, bf16[4096,128]{1,0:T(8,128)(2,1)}, u32[]{:S(2)}) %copy-start.1) | copy-done | bytes 1048600
  3.8 0.0 copy-start.2
  3.8 1.2 %copy-done.2 = bf16[4096,128]{1,0:T(8,128)(2,1)S(1)} copy-done((bf16[4096,128]{1,0:T(8,128)(2,1)S(1)}, bf16[4096,128]{1,0:T(8,128)(2,1)}, u32[]{:S(2)}) %copy-start.2) | copy-done | bytes 1048600
  5.0 0.0 copy-start.3
  5.0 1.0 %copy-done.3 = bf16[3,512,128]{2,1,0:T(8,128)(2,1)S(1)} copy-done((bf16[3,512,128]{2,1,0:T(8,128)(2,1)S(1)}, bf16[3,512,128]{2,1,0:T(8,128)(2,1)}, u32[]{:S(2)}) %copy-start.3) | copy-done | bytes 393240
  6.0 90.9 %shard_map.77 = (bf16[3,2,4,64]{3,2,1,0:T(4,128)(2,1)S(1)}, bf16[3,128]{1,0:T(4,128)(2,1)S(1)}) custom-call(bf16[3,512,128]{2,1,0:T(8,128)(2,1)S(1)} %copy-done.3, bf16[3,1,128]{2,1,0:T(2,128)(2,1)S(1)} %copy.8.new_ref, bf16[4096,128]{1,0:T(8,128)(2,1)S(1)} %copy-done, bf16[4096,128]{1,0:T(8,128)(2,1)S(1)} %copy-done.1, bf16[4096,128]{1,0:T(8,128)(2,1)S(1)} %copy-done.2, ...), custom_call_target="tpu_custom_call" | custom-call | tf_op jit(solution)/shard_map/pallas_call | solution.py:362
  96.9 0.6 copy.11
  97.5 0.6 copy.12
Async XLA Ops:
  0.6 0.7 copy-start.4
  1.3 1.2 %copy-start = (bf16[4096,128]{1,0:T(8,128)(2,1)S(1)}, bf16[4096,128]{1,0:T(8,128)(2,1)}, u32[]{:S(2)}) copy-start(bf16[4096,128]{1,0:T(8,128)(2,1)} %wq_ref.1) | copy-start | bytes 3145732
  2.6 1.2 %copy-start.1 = (bf16[4096,128]{1,0:T(8,128)(2,1)S(1)}, bf16[4096,128]{1,0:T(8,128)(2,1)}, u32[]{:S(2)}) copy-start(bf16[4096,128]{1,0:T(8,128)(2,1)} %wk_ref.1) | copy-start | bytes 3145732
  3.8 1.2 %copy-start.2 = (bf16[4096,128]{1,0:T(8,128)(2,1)S(1)}, bf16[4096,128]{1,0:T(8,128)(2,1)}, u32[]{:S(2)}) copy-start(bf16[4096,128]{1,0:T(8,128)(2,1)} %wv_ref.1) | copy-start | bytes 3145732
  5.0 1.0 %copy-start.3 = (bf16[3,512,128]{2,1,0:T(8,128)(2,1)S(1)}, bf16[3,512,128]{2,1,0:T(8,128)(2,1)}, u32[]{:S(2)}) copy-start(bf16[3,512,128]{2,1,0:T(8,128)(2,1)} %tok_ref.1) | copy-start | bytes 1179652

commit v2 on v1

--- a/solution.py
+++ b/solution.py
@@ -91,7 +91,7 @@
         )
 
     own_new = jnp.concatenate(
-        [new_ref[:, 0, :].astype(jnp.float32), jnp.zeros((13, LANES), jnp.float32)], axis=0
+        [new_ref[...].astype(jnp.float32), jnp.zeros((13, LANES), jnp.float32)], axis=0
     )
     news[tp] = own_new.astype(jnp.bfloat16)
 
@@ -299,43 +299,44 @@
         tile = jnp.where(low, total[0:HD, :], total[HD:, :]) * carried
         query = jnp.where(low, q_cols[0:HD, p : p + 1], q_cols[HD:, p : p + 1])
         partial = jnp.sum(tile * query, axis=0, keepdims=True) * one
-        out_buf[:, pl.ds(p * 4, 4), :] = tile.reshape(groups, HD // groups, LANES)
-        out_buf[:, pl.ds(12 + p, 1), :] = jnp.broadcast_to(partial[None], (groups, 1, LANES))
-
-    out_buf[:, pl.ds(15, 1), :] = jnp.zeros((groups, 1, LANES), jnp.float32)
+        out_buf[p, :, pl.ds(0, 4), :] = tile.reshape(groups, HD // groups, LANES)
+        out_buf[p, :, pl.ds(4, 1), :] = jnp.broadcast_to(partial[None], (groups, 1, LANES))
+        in_buf[p, sp] = out_buf[p, sp]
+        for d in range(1, groups):
+            peer = (sp + d) % groups
+            pltpu.make_async_remote_copy(
+                src_ref=out_buf.at[p, peer],
+                dst_ref=in_buf.at[p, sp],
+                send_sem=x_send.at[p],
+                recv_sem=x_recv.at[p],
+                device_id=(peer, tp),
+                device_id_type=MESH,
+            ).start()
+
+    def arrived(p):
+        view = in_buf.at[p, pl.ds(0, groups - 1)]
+        pltpu.make_async_copy(view, view, x_recv.at[p]).wait()
+        parts = [in_buf[p, d] for d in range(groups)]
+        while len(parts) > 1:
+            parts = [parts[i] + parts[i + 1] for i in range(0, len(parts), 2)]
+        whole = parts[0]
+        rows = whole[0:4, :].astype(jnp.bfloat16)
+        state_ref[p, 0] = rows[:, 0:HD]
+        state_ref[p, 1] = rows[:, HD:]
+        raw = whole[4:5, :] + own_term[p : p + 1, :]
+        centered = raw - head_sums(raw) * (1.0 / HD)
+        scale = lax.rsqrt(head_sums(centered * centered) * (1.0 / HD) + 1e-05)
+        read_ref[pl.ds(p, 1), :] = (centered * scale).astype(jnp.bfloat16)
+
+    out_buf[:, :, pl.ds(5, 3), :] = jnp.zeros((3, groups, 3, LANES), jnp.float32)
     finish(0)
     relay(last + 2)
     compute(last + 1)
     finish(1)
     compute(last + 2)
     finish(2)
-
-    for d in range(1, groups):
-        peer = (sp + d) % groups
-        pltpu.make_async_remote_copy(
-            src_ref=out_buf.at[peer],
-            dst_ref=in_buf.at[sp],
-            send_sem=x_send,
-            recv_sem=x_recv,
-            device_id=(peer, tp),
-            device_id_type=MESH,
-        ).start()
-    pltpu.make_async_copy(
-        in_buf.at[pl.ds(0, groups - 1)], in_buf.at[pl.ds(0, groups - 1)], x_recv
-    ).wait()
-    in_buf[sp] = out_buf[sp]
-    whole = in_buf[0]
-    for d in range(1, groups):
-        whole = whole + in_buf[d]
-
     for p in range(3):
-        rows = whole[p * 4 : p * 4 + 4, :].astype(jnp.bfloat16)
-        state_ref[p, 0] = rows[:, 0:HD]
-        state_ref[p, 1] = rows[:, HD:]
-    raw = whole[12:15, :] + own_term[0:3, :]
-    centered = raw - head_sums(raw) * (1.0 / HD)
-    scale = lax.rsqrt(head_sums(centered * centered) * (1.0 / HD) + 1e-05)
-    read_ref[...] = (centered * scale).astype(jnp.bfloat16)
+        arrived(p)
 
     def drain(view, sem):
         pltpu.make_async_copy(view, view, sem).wait()
@@ -349,7 +350,8 @@
         drain(news.at[0], nd_send.at[k])
     for k in range(16):
         drain(news.at[0], np_send.at[k])
-    drain(in_buf.at[pl.ds(0, groups - 1)], x_send)
+    for p in range(3):
+        drain(in_buf.at[p, pl.ds(0, groups - 1)], x_send.at[p])
 
 
 def body(tokens, new_token, query_weight, key_weight, value_weight, log_decay):
@@ -357,7 +359,7 @@
     n_tp = lax.axis_size("tp")
     depth = n_tp * LANES
     dma = pltpu.SemaphoreType.DMA
-    anywhere = pl.BlockSpec(memory_space=pl.ANY)
+    anywhere = pl.BlockSpec(memory_space=pltpu.HBM)
     vmem = pl.BlockSpec(memory_space=pltpu.VMEM)
     return pl.pallas_call(
         functools.partial(kernel, groups),
@@ -383,8 +385,8 @@
             pltpu.VMEM((2 * CH, LANES), jnp.float32),
             pltpu.VMEM((2 * CH, LANES), jnp.float32),
             pltpu.VMEM((2 * CH, LANES), jnp.float32),
-            pltpu.VMEM((groups, 16, LANES), jnp.float32),
-            pltpu.VMEM((groups, 16, LANES), jnp.float32),
+            pltpu.VMEM((3, groups, 8, LANES), jnp.float32),
+            pltpu.VMEM((3, groups, 8, LANES), jnp.float32),
             dma((NCH,)),
             dma((3,)),
             dma,
@@ -403,13 +405,13 @@
             dma((8,)),
             dma((7,)),
             dma,
-            dma,
-            dma,
+            dma((3,)),
+            dma((3,)),
         ],
         compiler_params=pltpu.CompilerParams(
-            collective_id=0, has_side_effects=True, vmem_limit_bytes=48 * 1024 * 1024
+            collective_id=0, has_side_effects=True, vmem_limit_bytes=55112 * 1024
         ),
-    )(tokens, new_token, query_weight, key_weight, value_weight, log_decay)
+    )(tokens, new_token[:, 0, :], query_weight, key_weight, value_weight, log_decay)
 
 
 def solution(mesh):

time: 98.4 us -> 92.4 us (0.939)
  local copies, waits for them, and re-layouts: 6.52 us -> 1.84 us
  Pallas kernels: 90.9 us -> 89.8 us
    unnamed x13 -> x6, local copies, waits for them, and re-layouts: 6.52 us -> 1.84 us
    pallas_call x1, Pallas kernels: 90.9 us -> 89.8 us  [body(): pl.pallas_call(functools.partial(kernel, groups), out_shape=(jax.ShapeDty...]
where the time goes in v2:
time: 92.4 us; the launch traced here: 92.3 us
  Pallas kernels  89.8 us (97%)
  local copies, waits for them, and re-layouts  1.84 us (2%)
    pallas_call x1, Pallas kernels, body(): pl.pallas_call(functools.partial(kernel, groups), out_shape=(jax.ShapeDty...  89.8 us

profile of v2, /device:TPU:1, one launch (start us, length us, event | category | flops | bytes accessed | tf_op | source)
XLA Modules:
  0.0 92.3 jit_solution(17958746084819590713)
XLA Ops:
  0.6 0.0 copy-start.1
  0.6 0.0 copy-start
  0.7 0.6 copy-done.1
  1.3 0.0 copy-done
  1.3 89.8 %shard_map.77 = (bf16[3,2,4,64]{3,2,1,0:T(4,128)(2,1)S(1)}, bf16[3,128]{1,0:T(4,128)(2,1)S(1)}) custom-call(bf16[3,512,128]{2,1,0:T(8,128)(2,1)} %tok_ref.1, bf16[3,128]{1,0:T(4,128)(2,1)S(1)} %bitcast.1, bf16[4096,128]{1,0:T(8,128)(2,1)} %wq_ref.1, bf16[4096,128]{1,0:T(8,128)(2,1)} %wk_ref.1, bf16[4096,128]{1,0:T(8,128)(2,1)} %wv_ref.1, f32[2]{0:T(128)S(1)} %copy-done.1), custom_call_target="tpu_custom_call" | custom-call | tf_op jit(solution)/shard_map/pallas_call | solution.py:364
  91.1 0.6 copy.10
  91.7 0.6 copy.11
Async XLA Ops:
  0.6 0.7 copy-start.1
  0.6 0.7 copy-start

commit v3 on v2

--- a/solution.py
+++ b/solution.py
@@ -58,10 +58,12 @@
     nown_recv,
     x_send,
     x_recv,
+    ready,
 ):
     sp = lax.axis_index("sp")
     tp = lax.axis_index("tp")
     z = tp // 2
+    y, x = sp // 4, sp % 4
     core = tp % 2
     up = ((z + 1) % NZ) * 2 + core
     dn = ((z + NZ - 1) % NZ) * 2 + core
@@ -85,17 +87,25 @@
     barrier = pltpu.get_barrier_semaphore()
     for peer in (up, dn, partner):
         pl.semaphore_signal(barrier, inc=1, device_id=(sp, peer), device_id_type=MESH)
-    for d in range(1, groups):
-        pl.semaphore_signal(
-            barrier, inc=1, device_id=((sp + d) % groups, tp), device_id_type=MESH
-        )
+    beside = [y * 4 + (x + d) % 4 for d in (1, 3)] + [((y + d) % 4) * 4 + x for d in (1, 3)]
+    for peer in beside:
+        pl.semaphore_signal(barrier, inc=1, device_id=(peer, tp), device_id_type=MESH)
 
     own_new = jnp.concatenate(
-        [new_ref[...].astype(jnp.float32), jnp.zeros((13, LANES), jnp.float32)], axis=0
+        [new_ref[...].astype(jnp.float32), jnp.zeros((5, LANES), jnp.float32)], axis=0
     )
     news[tp] = own_new.astype(jnp.bfloat16)
 
-    pl.semaphore_wait(barrier, 3 + groups - 1)
+    pl.semaphore_wait(barrier, 3 + 4)
+
+    def tell(r):
+        for peer in beside:
+            pl.semaphore_signal(ready.at[r], inc=1, device_id=(peer, tp), device_id_type=MESH)
+
+    def told(r):
+        pl.semaphore_wait(ready.at[r], 4)
+
+    tell(0)
 
     def remote(src, send, recv, peer, ref=None):
         ref = blocks if ref is None else ref
@@ -145,6 +155,8 @@
     dec_t[...] = jnp.exp((span - 1 - row).astype(jnp.float32) * ld)
     carried = jnp.exp(ld * (span * (groups - 1 - sp)).astype(jnp.float32))
 
+    told(0)
+    tell(1)
     for c in w_copies:
         c.wait()
 
@@ -170,6 +182,9 @@
     for ch in range(NCH):
         remote(partner * NCH + ch, pt_send, own_recv.at[ch], partner).wait_recv()
         acc[pl.ds(ch * CH, CH), :] = kv_dot(z, ch)
+
+    told(1)
+    tell(2)
 
     def relay(t):
         k, su, cu = source(t, False)
@@ -261,6 +276,7 @@
         swapped = jnp.where(first, pltpu.roll(x, LANES - 32, 1), pltpu.roll(x, 32, 1))
         return x * cosine + swapped * sine
 
+    told(2)
     relay(last + 1)
     compute(last)
 
@@ -299,8 +315,12 @@
         tile = jnp.where(low, total[0:HD, :], total[HD:, :]) * carried
         query = jnp.where(low, q_cols[0:HD, p : p + 1], q_cols[HD:, p : p + 1])
         partial = jnp.sum(tile * query, axis=0, keepdims=True) * one
-        out_buf[p, :, pl.ds(0, 4), :] = tile.reshape(groups, HD // groups, LANES)
-        out_buf[p, :, pl.ds(4, 1), :] = jnp.broadcast_to(partial[None], (groups, 1, LANES))
+        packed = [
+            tile.reshape(groups, HD // groups, LANES),
+            jnp.broadcast_to(partial[None], (groups, 1, LANES)),
+            jnp.zeros((groups, 3, LANES), jnp.float32),
+        ]
+        out_buf[p] = jnp.concatenate(packed, axis=1).astype(jnp.bfloat16)
         in_buf[p, sp] = out_buf[p, sp]
         for d in range(1, groups):
             peer = (sp + d) % groups
@@ -316,7 +336,7 @@
     def arrived(p):
         view = in_buf.at[p, pl.ds(0, groups - 1)]
         pltpu.make_async_copy(view, view, x_recv.at[p]).wait()
-        parts = [in_buf[p, d] for d in range(groups)]
+        parts = [in_buf[p, d].astype(jnp.float32) for d in range(groups)]
         while len(parts) > 1:
             parts = [parts[i] + parts[i + 1] for i in range(0, len(parts), 2)]
         whole = parts[0]
@@ -328,7 +348,6 @@
         scale = lax.rsqrt(head_sums(centered * centered) * (1.0 / HD) + 1e-05)
         read_ref[pl.ds(p, 1), :] = (centered * scale).astype(jnp.bfloat16)
 
-    out_buf[:, :, pl.ds(5, 3), :] = jnp.zeros((3, groups, 3, LANES), jnp.float32)
     finish(0)
     relay(last + 2)
     compute(last + 1)
@@ -378,15 +397,15 @@
         out_specs=(vmem, vmem),
         scratch_shapes=[
             pltpu.VMEM((n_tp * NCH, CH, LANES), jnp.bfloat16),
-            pltpu.VMEM((n_tp, 16, LANES), jnp.bfloat16),
+            pltpu.VMEM((n_tp, 8, LANES), jnp.bfloat16),
             pltpu.VMEM((depth, 3 * LANES), jnp.bfloat16),
             pltpu.VMEM((NCH * CH, 2 * LANES), jnp.float32),
-            pltpu.VMEM((16, 3 * LANES), jnp.float32),
+            pltpu.VMEM((8, 3 * LANES), jnp.float32),
             pltpu.VMEM((2 * CH, LANES), jnp.float32),
             pltpu.VMEM((2 * CH, LANES), jnp.float32),
             pltpu.VMEM((2 * CH, LANES), jnp.float32),
-            pltpu.VMEM((3, groups, 8, LANES), jnp.float32),
-            pltpu.VMEM((3, groups, 8, LANES), jnp.float32),
+            pltpu.VMEM((3, groups, 8, LANES), jnp.bfloat16),
+            pltpu.VMEM((3, groups, 8, LANES), jnp.bfloat16),
             dma((NCH,)),
             dma((3,)),
             dma,
@@ -407,6 +426,7 @@
             dma,
             dma((3,)),
             dma((3,)),
+            pltpu.SemaphoreType.REGULAR((3,)),
         ],
         compiler_params=pltpu.CompilerParams(
             collective_id=0, has_side_effects=True, vmem_limit_bytes=55112 * 1024

time: 92.4 us -> 91.6 us (level)
  no operation moved by 1% of the time
where the time goes in v3:
time: 91.6 us; the launch traced here: 91.5 us
  Pallas kernels  89 us (97%)
  local copies, waits for them, and re-layouts  1.84 us (2%)
    pallas_call x1, Pallas kernels, body(): pl.pallas_call(functools.partial(kernel, groups), out_shape=(jax.ShapeDty...  89 us
    unnamed x6, local copies, waits for them, and re-layouts  1.84 us

profile of v3, /device:TPU:1, one launch (start us, length us, event | category | flops | bytes accessed | tf_op | source)
XLA Modules:
  0.0 91.5 jit_solution(4850170102349082846)
XLA Ops:
  0.6 0.0 copy-start.1
  0.6 0.0 copy-start
  0.7 0.6 copy-done.1
  1.3 0.0 copy-done
  1.3 89.0 %shard_map.77 = (bf16[3,2,4,64]{3,2,1,0:T(4,128)(2,1)S(1)}, bf16[3,128]{1,0:T(4,128)(2,1)S(1)}) custom-call(bf16[3,512,128]{2,1,0:T(8,128)(2,1)} %tok_ref.1, bf16[3,128]{1,0:T(4,128)(2,1)S(1)} %bitcast.1, bf16[4096,128]{1,0:T(8,128)(2,1)} %wq_ref.1, bf16[4096,128]{1,0:T(8,128)(2,1)} %wk_ref.1, bf16[4096,128]{1,0:T(8,128)(2,1)} %wv_ref.1, f32[2]{0:T(128)S(1)} %copy-done.1), custom_call_target="tpu_custom_call" | custom-call | tf_op jit(solution)/shard_map/pallas_call | solution.py:383
  90.3 0.6 copy.10
  90.9 0.6 copy.11
Async XLA Ops:
  0.6 0.7 copy-start.1
  0.6 0.7 copy-start

commit v4 on v3

--- a/solution.py
+++ b/solution.py
@@ -12,10 +12,15 @@
 MESH = pl.DeviceIdType.MESH
 NZ = 16
 CH = 256
-NCH = 6
-HALF = 3
+PARTS = 2
+NCH = 3 * PARTS
+HALF = NCH // 2
 STEPS = 7 * NCH + HALF
 LANES = 128
+OTHERS = sorted(
+    ((dy, dx) for dy in range(4) for dx in range(4) if dy or dx),
+    key=lambda d: -sum(min(v, 4 - v) for v in d),
+)
 
 
 def kernel(
@@ -68,13 +73,20 @@
     up = ((z + 1) % NZ) * 2 + core
     dn = ((z + NZ - 1) % NZ) * 2 + core
     partner = z * 2 + (1 - core)
-    span = NCH // 3 * CH
+    span = PARTS * CH
+
+    barrier = pltpu.get_barrier_semaphore()
+    for peer in (up, dn, partner):
+        pl.semaphore_signal(barrier, inc=1, device_id=(sp, peer), device_id_type=MESH)
+    beside = [y * 4 + (x + d) % 4 for d in (1, 3)] + [((y + d) % 4) * 4 + x for d in (1, 3)]
+    for peer in beside:
+        pl.semaphore_signal(barrier, inc=1, device_id=(peer, tp), device_id_type=MESH)
 
     own_copies = []
     for ch in range(NCH):
-        half, p = ch // 3, ch % 3
+        part, p = ch // 3, ch % 3
         c = pltpu.make_async_copy(
-            tok_ref.at[p, pl.ds(half * CH, CH), :], blocks.at[tp * NCH + ch], tok_sem.at[ch]
+            tok_ref.at[p, pl.ds(part * CH, CH), :], blocks.at[tp * NCH + ch], tok_sem.at[ch]
         )
         c.start()
         own_copies.append(c)
@@ -83,13 +95,6 @@
         c = pltpu.make_async_copy(ref, weights.at[:, pl.ds(i * LANES, LANES)], w_sem.at[i])
         c.start()
         w_copies.append(c)
-
-    barrier = pltpu.get_barrier_semaphore()
-    for peer in (up, dn, partner):
-        pl.semaphore_signal(barrier, inc=1, device_id=(sp, peer), device_id_type=MESH)
-    beside = [y * 4 + (x + d) % 4 for d in (1, 3)] + [((y + d) % 4) * 4 + x for d in (1, 3)]
-    for peer in beside:
-        pl.semaphore_signal(barrier, inc=1, device_id=(peer, tp), device_id_type=MESH)
 
     own_new = jnp.concatenate(
         [new_ref[...].astype(jnp.float32), jnp.zeros((5, LANES), jnp.float32)], axis=0
@@ -121,10 +126,11 @@
     remote(tp, nu_send.at[0], nu_recv.at[0], up, news).start()
     remote(tp, nd_send.at[0], nd_recv.at[0], dn, news).start()
     remote(tp, np_send.at[15], nown_recv, partner, news).start()
-    for ch in range(NCH):
-        own_copies[ch].wait()
     for pos in range(NCH):
         cu, cd = pos, (pos + HALF) % NCH
+        if pos < HALF:
+            own_copies[cu].wait()
+            own_copies[cd].wait()
         remote(tp * NCH + cu, up_send, up_recv.at[pos], up).start()
         remote(tp * NCH + cd, dn_send, dn_recv.at[pos], dn).start()
     for ch in range(NCH):
@@ -147,7 +153,7 @@
         inverse = jnp.where(lane % 32 == i, float(freq[i]), inverse)
     first = (lane % HD) < 32
     low = lane < HD
-    ld = jnp.where(low, ld_ref[0], ld_ref[1])
+    ld = jnp.where(low, ld_ref[0:1, 0:1], ld_ref[0:1, 1:2])
     row = lax.broadcasted_iota(jnp.int32, (span, LANES), 0)
     angle = (row + sp * span).astype(jnp.float32) * inverse
     cos_t[...] = jnp.cos(angle) * 0.125
@@ -277,41 +283,37 @@
         return x * cosine + swapped * sine
 
     told(2)
-    relay(last + 1)
-    compute(last)
-
-    new_angle = (groups * span) * inverse
-    new_cos = jnp.cos(new_angle)
-    new_sin = jnp.where(first, -jnp.sin(new_angle), jnp.sin(new_angle))
-    new_k = (turned(acc_new[0:8, 0:128], new_cos, new_sin) * 0.125).astype(jnp.bfloat16)
-    new_v = acc_new[0:8, 128:256].astype(jnp.bfloat16).astype(jnp.float32)
-    new_q = turned(acc_new[0:8, 256:384], new_cos, new_sin).astype(jnp.bfloat16)
-    new_q = new_q.astype(jnp.float32)
-    product = new_q * new_k.astype(jnp.float32)
-
-    def head_sums(x):
-        lo = jnp.sum(jnp.where(low, x, 0.0), axis=1, keepdims=True)
-        hi = jnp.sum(jnp.where(low, 0.0, x), axis=1, keepdims=True)
+
+    def head_sums(v):
+        lo = jnp.sum(jnp.where(low, v, 0.0), axis=1, keepdims=True)
+        hi = jnp.sum(jnp.where(low, 0.0, v), axis=1, keepdims=True)
         return jnp.where(low, lo, hi)
 
-    own_term = head_sums(product) * new_v
-    q_cols = jnp.transpose(jnp.concatenate([new_q] * 16, axis=0))
     one = jnp.exp(ld)
 
-    def finish(p):
-        total = None
-        for half in range(2):
-            at = pl.ds(half * CH, CH)
-            rows = acc[pl.ds((half * 3 + p) * CH, CH), :]
-            keys = turned(rows[:, 0:128], cos_t[at, :], sin_t[at, :]).astype(jnp.bfloat16)
-            keys = (keys.astype(jnp.float32) * dec_t[at, :]).astype(jnp.bfloat16)
-            part = lax.dot_general(
-                keys,
-                rows[:, 128:256].astype(jnp.bfloat16),
-                (((0,), (0,)), ((), ())),
-                preferred_element_type=jnp.float32,
-            )
-            total = part if total is None else total + part
+    def query_of_new():
+        new_angle = (groups * span) * inverse
+        new_cos = jnp.cos(new_angle)
+        new_sin = jnp.where(first, -jnp.sin(new_angle), jnp.sin(new_angle))
+        new_k = (turned(acc_new[0:8, 0:128], new_cos, new_sin) * 0.125).astype(jnp.bfloat16)
+        new_v = acc_new[0:8, 128:256].astype(jnp.bfloat16).astype(jnp.float32)
+        new_q = turned(acc_new[0:8, 256:384], new_cos, new_sin).astype(jnp.bfloat16)
+        new_q = new_q.astype(jnp.float32)
+        return new_q, head_sums(new_q * new_k.astype(jnp.float32)) * new_v
+
+    def part_of(p, part):
+        at = pl.ds(part * CH, CH)
+        rows = acc[pl.ds((part * 3 + p) * CH, CH), :]
+        keys = turned(rows[:, 0:128], cos_t[at, :], sin_t[at, :]).astype(jnp.bfloat16)
+        keys = (keys.astype(jnp.float32) * dec_t[at, :]).astype(jnp.bfloat16)
+        return lax.dot_general(
+            keys,
+            rows[:, 128:256].astype(jnp.bfloat16),
+            (((0,), (0,)), ((), ())),
+            preferred_element_type=jnp.float32,
+        )
+
+    def hand_out(p, total):
         tile = jnp.where(low, total[0:HD, :], total[HD:, :]) * carried
         query = jnp.where(low, q_cols[0:HD, p : p + 1], q_cols[HD:, p : p + 1])
         partial = jnp.sum(tile * query, axis=0, keepdims=True) * one
@@ -321,9 +323,8 @@
             jnp.zeros((groups, 3, LANES), jnp.float32),
         ]
         out_buf[p] = jnp.concatenate(packed, axis=1).astype(jnp.bfloat16)
-        in_buf[p, sp] = out_buf[p, sp]
-        for d in range(1, groups):
-            peer = (sp + d) % groups
+        for dy, dx in OTHERS:
+            peer = ((y + dy) % 4) * 4 + (x + dx) % 4
             pltpu.make_async_remote_copy(
                 src_ref=out_buf.at[p, peer],
                 dst_ref=in_buf.at[p, sp],
@@ -332,6 +333,7 @@
                 device_id=(peer, tp),
                 device_id_type=MESH,
             ).start()
+        in_buf[p, sp] = out_buf[p, sp]
 
     def arrived(p):
         view = in_buf.at[p, pl.ds(0, groups - 1)]
@@ -348,12 +350,19 @@
         scale = lax.rsqrt(head_sums(centered * centered) * (1.0 / HD) + 1e-05)
         read_ref[pl.ds(p, 1), :] = (centered * scale).astype(jnp.bfloat16)
 
-    finish(0)
-    relay(last + 2)
-    compute(last + 1)
-    finish(1)
-    compute(last + 2)
-    finish(2)
+    totals = [None] * 3
+    for pos in range(HALF):
+        if pos + 1 < HALF:
+            relay(last + pos + 1)
+        compute(last + pos)
+        if pos == 0:
+            new_q, own_term = query_of_new()
+            q_cols = jnp.transpose(jnp.concatenate([new_q] * 16, axis=0))
+        p, part = pos % 3, pos // 3
+        both = part_of(p, part) + part_of(p, part + PARTS // 2)
+        totals[p] = both if totals[p] is None else totals[p] + both
+        if part == PARTS // 2 - 1:
+            hand_out(p, totals[p])
     for p in range(3):
         arrived(p)
 
@@ -392,7 +401,7 @@
             anywhere,
             anywhere,
             anywhere,
-            pl.BlockSpec(memory_space=pltpu.SMEM),
+            vmem,
         ],
         out_specs=(vmem, vmem),
         scratch_shapes=[
@@ -401,9 +410,9 @@
             pltpu.VMEM((depth, 3 * LANES), jnp.bfloat16),
             pltpu.VMEM((NCH * CH, 2 * LANES), jnp.float32),
             pltpu.VMEM((8, 3 * LANES), jnp.float32),
-            pltpu.VMEM((2 * CH, LANES), jnp.float32),
-            pltpu.VMEM((2 * CH, LANES), jnp.float32),
-            pltpu.VMEM((2 * CH, LANES), jnp.float32),
+            pltpu.VMEM((PARTS * CH, LANES), jnp.float32),
+            pltpu.VMEM((PARTS * CH, LANES), jnp.float32),
+            pltpu.VMEM((PARTS * CH, LANES), jnp.float32),
             pltpu.VMEM((3, groups, 8, LANES), jnp.bfloat16),
             pltpu.VMEM((3, groups, 8, LANES), jnp.bfloat16),
             dma((NCH,)),
@@ -431,7 +440,7 @@
         compiler_params=pltpu.CompilerParams(
             collective_id=0, has_side_effects=True, vmem_limit_bytes=55112 * 1024
         ),
-    )(tokens, new_token[:, 0, :], query_weight, key_weight, value_weight, log_decay)
+    )(tokens, new_token[:, 0, :], query_weight, key_weight, value_weight, log_decay[None])
 
 
 def solution(mesh):

time: 91.6 us -> 90.4 us (0.987)
  Pallas kernels: 89 us -> 87.8 us
    pallas_call x1, Pallas kernels: 89 us -> 87.8 us  [body(): pl.pallas_call(functools.partial(kernel, groups), out_shape=(jax.ShapeDty...]
where the time goes in v4:
time: 90.4 us; the launch traced here: 90.3 us
  Pallas kernels  87.8 us (97%)
  local copies, waits for them, and re-layouts  1.82 us (2%)
    pallas_call x1, Pallas kernels, body(): pl.pallas_call(functools.partial(kernel, groups), out_shape=(jax.ShapeDty...  87.8 us
    unnamed x6, local copies, waits for them, and re-layouts  1.82 us

profile of v4, /device:TPU:1, one launch (start us, length us, event | category | flops | bytes accessed | tf_op | source)
XLA Modules:
  0.0 90.3 jit_solution(923947420352944051)
XLA Ops:
  0.6 0.0 copy-start
  0.6 0.0 copy-start.1
  0.7 0.7 copy-done
  1.3 0.0 copy-done.1
  1.3 87.8 %shard_map.77 = (bf16[3,2,4,64]{3,2,1,0:T(4,128)(2,1)S(1)}, bf16[3,128]{1,0:T(4,128)(2,1)S(1)}) custom-call(bf16[3,512,128]{2,1,0:T(8,128)(2,1)} %tok_ref.1, bf16[3,128]{1,0:T(4,128)(2,1)S(1)} %bitcast.2, bf16[4096,128]{1,0:T(8,128)(2,1)} %wq_ref.1, bf16[4096,128]{1,0:T(8,128)(2,1)} %wk_ref.1, bf16[4096,128]{1,0:T(8,128)(2,1)} %wv_ref.1, f32[1,2]{1,0:T(1,128)S(1)} %bitcast.3), custom_call_target="tpu_custom_call" | custom-call | tf_op jit(solution)/shard_map/pallas_call | solution.py:392
  89.1 0.6 copy.10
  89.7 0.6 copy.11
Async XLA Ops:
  0.6 0.7 copy-start
  0.6 0.7 copy-start.1

commit v5 on v4

--- a/solution.py
+++ b/solution.py
@@ -301,9 +301,11 @@
         new_q = new_q.astype(jnp.float32)
         return new_q, head_sums(new_q * new_k.astype(jnp.float32)) * new_v
 
-    def part_of(p, part):
+    def part_of(p, part, added=None):
         at = pl.ds(part * CH, CH)
         rows = acc[pl.ds((part * 3 + p) * CH, CH), :]
+        if added is not None:
+            rows = rows + added
         keys = turned(rows[:, 0:128], cos_t[at, :], sin_t[at, :]).astype(jnp.bfloat16)
         keys = (keys.astype(jnp.float32) * dec_t[at, :]).astype(jnp.bfloat16)
         return lax.dot_general(
@@ -354,6 +356,17 @@
     for pos in range(HALF):
         if pos + 1 < HALF:
             relay(last + pos + 1)
+        if pos == HALF - 1:
+            t = last + pos
+            _, su, cu = source(t, False)
+            _, sd, cd = source(t, True)
+            other = 1 - core
+            remote((su * 2 + other) * NCH + cu, pt_send, pu_recv.at[t], partner).wait_recv()
+            total = totals[2] if totals[2] is not None else 0.0
+            total = total + part_of(2, cu // 3, kv_dot(su, cu))
+            remote((sd * 2 + other) * NCH + cd, pt_send, pd_recv.at[t], partner).wait_recv()
+            hand_out(2, total + part_of(2, cd // 3, kv_dot(sd, cd)))
+            continue
         compute(last + pos)
         if pos == 0:
             new_q, own_term = query_of_new()

time: 90.4 us -> 90.5 us (level)
  no operation moved by 1% of the time
where the time goes in v5:
time: 90.5 us; the launch traced here: 90.4 us
  Pallas kernels  87.9 us (97%)
  local copies, waits for them, and re-layouts  1.82 us (2%)
    pallas_call x1, Pallas kernels, body(): pl.pallas_call(functools.partial(kernel, groups), out_shape=(jax.ShapeDty...  87.9 us
    unnamed x6, local copies, waits for them, and re-layouts  1.82 us

profile of v5, /device:TPU:1, one launch (start us, length us, event | category | flops | bytes accessed | tf_op | source)
XLA Modules:
  0.0 90.4 jit_solution(5190585367009928561)
XLA Ops:
  0.6 0.0 copy-start
  0.6 0.0 copy-start.1
  0.7 0.7 copy-done
  1.3 0.0 copy-done.1
  1.3 87.9 %shard_map.77 = (bf16[3,2,4,64]{3,2,1,0:T(4,128)(2,1)S(1)}, bf16[3,128]{1,0:T(4,128)(2,1)S(1)}) custom-call(bf16[3,512,128]{2,1,0:T(8,128)(2,1)} %tok_ref.1, bf16[3,128]{1,0:T(4,128)(2,1)S(1)} %bitcast.2, bf16[4096,128]{1,0:T(8,128)(2,1)} %wq_ref.1, bf16[4096,128]{1,0:T(8,128)(2,1)} %wk_ref.1, bf16[4096,128]{1,0:T(8,128)(2,1)} %wv_ref.1, f32[1,2]{1,0:T(1,128)S(1)} %bitcast.3), custom_call_target="tpu_custom_call" | custom-call | tf_op jit(solution)/shard_map/pallas_call | solution.py:405
  89.2 0.6 copy.10
  89.8 0.6 copy.11
Async XLA Ops:
  0.6 0.7 copy-start
  0.6 0.7 copy-start.1
